TPU v7x, 128 devices: a whole 4x4x4 slice. The times are simulated.
128 devices in a mesh: rep: 2 (over z_hi), fs: 32 (over z_lo, y, x), tp: 2 (over core).
Axes of the slice: x: 4, y: 4, z: 4 (z_hi: 2, z_lo: 2; z = z_hi * 2 + z_lo), core: 2. Of those that a mesh axis runs over, the one named last changes fastest.
Arguments:
- hidden_in: bfloat16 [40960, 2048], P(('rep', 'fs'), 'tp'), may hold values from -6 to 6
- mix_gain: float32 [2048], replicated, may hold values from 0.1 to 1.9
- w_value: bfloat16 [2048, 1024], P('fs', 'tp'), may hold values from -0.125 to 0.125
- w_gate: bfloat16 [2048, 1024], P('fs', 'tp'), may hold values from -0.125 to 0.125
- conv_taps: float32 [31, 1024], P(None, 'tp'), may hold values from -5 to 5
- conv_bias: float32 [1024], P('tp'), may hold values from -3 to 3
- chan_gain: float32 [1024], P('tp'), may hold values from 0.1 to 1.9
- chan_bias: float32 [1024], P('tp'), may hold values from -3 to 3
- w_back: bfloat16 [1024, 2048], P('tp', 'fs'), may hold values from -0.1875 to 0.1875
- feed_gain: float32 [2048], replicated, may hold values from 0.1 to 1.9
- w_up: bfloat16 [2048, 8192], P(None, ('fs', 'tp')), may hold values from -0.125 to 0.125
- w_down: bfloat16 [8192, 2048], P(('fs', 'tp')), may hold values from -0.0625 to 0.0625
Outputs:
- layer_out: bfloat16 [40960, 2048], P(('rep', 'fs'), 'tp')
All inputs are finite; a program needn't handle non-finite values.
Results may differ from a plain program's by a relative error of at most 0.015.
Values may be sent and summed in bfloat16 or wider, within the bound.
A program may use at most 128 MiB of HBM per device.

v0:
```python
import jax
import jax.numpy as jnp
from jax import lax
from jax.sharding import PartitionSpec as P

KW = 31
LEN = 128


def copy_for_each(array, axis):
    copies = jnp.broadcast_to(array, (lax.axis_size(axis), *array.shape))
    return lax.all_to_all(copies, axis, split_axis=0, concat_axis=0, tiled=True)


def in_order(parts, dim):
    lengths = list(parts.shape[1:])
    lengths[dim] *= parts.shape[0]
    return jnp.moveaxis(parts, 0, dim).reshape(lengths)


def gathered_copies(array, axis, dim):
    parts = copy_for_each(array, axis)
    return in_order(parts, dim)


def side_by_side(arrays, axis, dim, along):
    widths = [a.shape[along] for a in arrays]
    both = jnp.concatenate(arrays, axis=along)
    result = lax.all_gather(both, axis, axis=dim, tiled=True)
    return tuple(jnp.split(result, [sum(widths[:k]) for k in range(1, len(widths))], axis=along))


def in_blocks(array, dim, count):
    lengths = array.shape
    parts = array.reshape(*lengths[:dim], count, lengths[dim] // count, *lengths[dim + 1 :])
    return jnp.moveaxis(parts, dim, 0)


def summed_on_arrival(array, axis, dim):
    count = lax.axis_size(axis)
    parts = lax.all_to_all(in_blocks(array, dim, count), axis, 0, 0, tiled=True)
    return jnp.sum(parts.astype(jnp.float32), axis=0)


def rms_norm(stream, gain):
    values = stream.astype(jnp.float32)
    scaled = values * lax.rsqrt(jnp.mean(values * values, axis=-1, keepdims=True) + 1e-06)
    return (scaled * gain).astype(jnp.bfloat16)


def causal_filter(gated, conv_taps, conv_bias):
    channels = gated.shape[1]
    blocks = gated.reshape(gated.shape[0] // LEN, LEN, channels)
    padded = jnp.pad(blocks, ((0, 0), (KW - 1, 0), (0, 0)))
    result = jnp.zeros_like(blocks) + conv_bias
    for tap_index in range(KW):
        result = result + conv_taps[tap_index] * padded[:, tap_index : tap_index + LEN]
    return result.reshape(gated.shape)


def shards(
    hidden_in,
    mix_gain,
    w_value,
    w_gate,
    conv_taps,
    conv_bias,
    chan_gain,
    chan_bias,
    w_back,
    feed_gain,
    w_up,
    w_down,
):
    gathered = gathered_copies(hidden_in, "tp", 1)
    normed = rms_norm(gathered, mix_gain)
    local_channels = w_value.shape[1]
    whole_value, whole_gate = side_by_side((w_value, w_gate), "fs", 0, 1)
    value_proj = jnp.dot(normed, whole_value, preferred_element_type=jnp.float32)
    gate_proj = jnp.dot(normed, whole_gate, preferred_element_type=jnp.float32)
    gated = value_proj * jax.nn.sigmoid(gate_proj)
    filtered = causal_filter(gated, conv_taps, conv_bias)
    channel_total = local_channels * lax.axis_size("tp")
    first_sum, square_sum = lax.psum(
        (jnp.sum(filtered, axis=1), jnp.sum(filtered * filtered, axis=1)), "tp"
    )
    chan_mean = (first_sum / channel_total)[:, None]
    chan_var = (square_sum / channel_total)[:, None] - chan_mean * chan_mean
    centred = (filtered - chan_mean) * lax.rsqrt(chan_var + 1e-05) * chan_gain + chan_bias
    mixer_act = jax.nn.silu(centred).astype(jnp.bfloat16)
    whole_back = gathered_copies(w_back, "fs", 1)
    partial_value = jnp.dot(mixer_act, whole_back, preferred_element_type=jnp.float32)
    summed = summed_on_arrival(partial_value.astype(jnp.bfloat16), "tp", 1)
    second = (hidden_in.astype(jnp.float32) + summed).astype(jnp.bfloat16)
    gathered_feed = lax.all_gather(second, "tp", axis=1, tiled=True)
    normed_feed = rms_norm(gathered_feed, feed_gain)
    up_proj = jnp.dot(
        normed_feed,
        lax.all_gather(w_up, "fs", axis=1, tiled=True),
        preferred_element_type=jnp.float32,
    )
    hidden = jnp.square(jax.nn.relu(up_proj)).astype(jnp.bfloat16)
    feed_partial = jnp.dot(
        hidden, lax.all_gather(w_down, "fs", axis=0, tiled=True), preferred_element_type=jnp.float32
    )
    feed = summed_on_arrival(feed_partial.astype(jnp.bfloat16), "tp", 1)
    return (second.astype(jnp.float32) + feed).astype(jnp.bfloat16)


def solution(mesh):
    placed = (
        P(("rep", "fs"), "tp"),
        P(),
        P("fs", "tp"),
        P("fs", "tp"),
        P(None, "tp"),
        P("tp"),
        P("tp"),
        P("tp"),
        P("tp", "fs"),
        P(),
        P(None, ("fs", "tp")),
        P(("fs", "tp"), None),
    )
    return jax.shard_map(
        shards, mesh=mesh, in_specs=placed, out_specs=P(("rep", "fs"), "tp"), check_vma=False
    )
```

profile of v0, /device:TPU:1, one launch (start us, length us, event | category | flops | bytes accessed | tf_op | source)
XLA Modules:
  0.0 708.8 jit_solution(11881618682649393780)
XLA Ops:
  6.5 0.0 all-gather.5.cloned.1.call-start
  6.5 1.5 pad_maximum_fusion
  8.1 0.0 all-gather.5.cloned.1.call-update
  8.1 1.7 copy.15
  9.8 0.2 broadcast_in_dim.4
  10.0 0.0 copy-start.5
  10.0 7.0 all_to_all.20
  17.0 0.0 copy-done.5
  17.0 1.6 broadcast_in_dim.5
  18.6 8.6 %all-to-all-start.1 = ((bf16[32,512,64]{1,2,0:T(8,128)(2,1)}), bf16[32,512,64]{1,2,0:T(8,128)(2,1)}, u32[]{:S(2)}, u32[]{:S(2)}) async-start(bf16[32,512,64]{1,2,0:T(8,128)(2,1)} %broadcast_in_dim.5), calls=%async_computation.1 | async-start | bytes 4194304 | tf_op jit(solution)/shard_map/all_to_all | solution.py:12
  27.3 0.0 copy-start.6
  27.3 0.0 copy-start.7
  27.3 0.0 all-gather.7.cloned.1.call-start
  27.3 0.6 multiply_reduce_fusion
  27.9 0.2 copy-done.6
  28.2 0.0 copy-done.7
  28.2 2.2 fusion.4
  30.4 0.0 copy-start.1
  30.4 127.4 %all-gather.5.cloned.1.call-done = bf16[2048,1024]{1,0:T(8,128)(2,1)} async-done(((bf16[64,1024]{1,0:T(8,128)(2,1)}), bf16[2048,1024]{1,0:T(8,128)(2,1)}) %all-gather.5.cloned.1.call-update) | async-done | bytes 4194320 | tf_op jit(solution)/shard_map/all_gather | solution.py:29
  157.8 0.0 copy-start.4
  157.8 4.2 fusion.28
  162.0 0.0 copy-done.1
  162.0 0.0 copy-done.4
  162.0 0.0 copy-start.8
  162.1 1.6 fusion.16
  163.6 0.0 copy-done.8
  163.7 0.0 copy-start.9
  163.7 0.0 copy-start.10
  163.7 5.5 fusion.93
  169.2 22.1 %all-reduce.1 = (f32[640]{0:T(1024)S(1)}, f32[640]{0:T(1024)S(1)}) all-reduce(f32[640]{0:T(1024)S(1)} %bitcast.77, f32[640]{0:T(1024)S(1)} %bitcast.76), channel_id=1, replica_groups=mesh['rep'=2,'fs'=32,'tp'=2] {'tp'}, use_global_device_ids=true, to_apply=%region_4.5 | all-reduce | flops 1280 | bytes 10240 | tf_op jit(solution)/shard_map/psum | solution.py:84
  191.2 0.0 copy-done.9
  191.2 0.0 copy-done.10
  191.2 0.5 multiply_convert_fusion.1
  191.8 0.0 all-to-all-done.1
  191.8 3.1 convolution_convert_fusion
  194.9 0.3 copy.23
  195.2 5.8 all_to_all.21
  201.0 0.0 copy-start.2
  201.0 0.6 convert_reduce_fusion.1
  201.6 0.7 copy-done.2
  202.3 1.5 add_convert_fusion.1
  203.9 0.0 all-gather.7.cloned.1.call-update
  203.9 0.0 all-gather.11.cloned.1.call-start
  204.0 0.7 all-gather.11.cloned.1.call-update
  204.6 0.2 all-gather.9.cloned.1.call-start
  204.9 0.3 all-gather.9.cloned.1.call-update
  205.2 0.0 copy-start.11
  205.2 13.4 %all-gather.7.cloned.1.call-done = bf16[640,2048]{1,0:T(8,128)(2,1)} async-done(((bf16[640,1024]{1,0:T(8,128)(2,1)}), bf16[640,2048]{1,0:T(8,128)(2,1)}) %all-gather.7.cloned.1.call-update) | async-done | bytes 2621456 | tf_op jit(solution)/shard_map/all_gather | solution.py:95
  218.7 0.0 copy-start.3
  218.7 2.5 fusion
  221.2 190.3 %all-gather.11.cloned.1.call-done = bf16[4096,2048]{1,0:T(8,128)(2,1)} async-done(((bf16[128,2048]{1,0:T(8,128)(2,1)}), bf16[4096,2048]{1,0:T(8,128)(2,1)}) %all-gather.11.cloned.1.call-update) | async-done | bytes 16777232 | tf_op jit(solution)/shard_map/all_gather | solution.py:104
  411.5 222.9 %all-gather.9.cloned.1.call-done = bf16[2048,4096]{1,0:T(8,128)(2,1)} async-done(((bf16[2048,128]{1,0:T(8,128)(2,1)}), bf16[2048,4096]{1,0:T(8,128)(2,1)}) %all-gather.9.cloned.1.call-update) | async-done | bytes 16777232 | tf_op jit(solution)/shard_map/all_gather | solution.py:99
  634.4 0.0 copy-done.11
  634.4 0.0 copy-done.3
  634.4 33.8 %convolution_convert_fusion.1 = bf16[640,2048]{1,0:T(8,128)(2,1)} fusion(bf16[4096,2048]{1,0:T(8,128)(2,1)} %all-gather.11.cloned.1.call-done, bf16[2048,4096]{1,0:T(8,128)(2,1)} %all-gather.9.cloned.1.call-done, bf16[640,2048]{1,0:T(8,128)(2,1)S(1)} %copy-done.3, f32[2048]{0:T(1024)S(1)} %copy-done.11, f32[640]{0:T(1024)S(1)} %add_rsqrt_fusion), kind=kOutput, calls=%fused_computation.43 | convolution fusion | flops 21489254400 | bytes 38808064 | tf_op jit(solution)/shard_map/dot_general | solution.py:103
  668.2 2.0 copy.22
  670.2 29.3 %all_to_all.22 = bf16[2,640,1024]{2,1,0:T(8,128)(2,1)S(1)} all-to-all(bf16[2,640,1024]{2,1,0:T(8,128)(2,1)S(1)} %bitcast.71), channel_id=1, replica_groups=mesh['rep'=2,'fs'=32,'tp'=2] {'tp'}, dimensions={0} | all-to-all | bytes 5242880 | tf_op jit(solution)/shard_map/all_to_all | solution.py:41
  699.4 0.0 copy-start
  699.4 0.6 convert_reduce_fusion
  700.0 0.7 copy-done
  700.8 1.5 add_convert_fusion
  (5 shorter events, 0.1 us)
Async XLA Ops:
  6.5 151.2 %all-gather.5.cloned.1.call-start = ((), (), s32[]{:S(2)}) async-start(), calls=%async_computation.4 | async-start | bytes 4325376 | tf_op jit(solution)/shard_map/all_gather | solution.py:29
  10.0 7.0 copy-start.5
  18.6 173.2 %all-to-all-start.1 = ((bf16[32,512,64]{1,2,0:T(8,128)(2,1)}), bf16[32,512,64]{1,2,0:T(8,128)(2,1)}, u32[]{:S(2)}, u32[]{:S(2)}) async-start(bf16[32,512,64]{1,2,0:T(8,128)(2,1)} %broadcast_in_dim.5), calls=%async_computation.1 | async-start | bytes 4194304 | tf_op jit(solution)/shard_map/all_to_all | solution.py:12
  27.3 0.8 copy-start.6
  27.3 0.9 copy-start.7
  27.3 191.4 %all-gather.7.cloned.1.call-start = ((), (), s32[]{:S(2)}) async-start(), calls=%async_computation.5 | async-start | bytes 3932160 | tf_op jit(solution)/shard_map/all_gather | solution.py:95
  30.4 131.7 %copy-start.1 = (bf16[640,2048]{0,1:T(8,128)(2,1)S(1)}, bf16[640,2048]{0,1:T(8,128)(2,1)}, u32[]{:S(2)}) copy-start(bf16[640,2048]{0,1:T(8,128)(2,1)} %fusion.4) | copy-start | bytes 7864324
  157.8 4.3 copy-start.4
  162.0 1.6 copy-start.8
  163.7 27.6 %copy-start.9 = (f32[512]{0:T(512)S(1)}, f32[512]{0:T(512)}, u32[]{:S(2)}) copy-start(f32[512]{0:T(512)} %param.19) | copy-start | bytes 6148
  163.7 27.6 %copy-start.10 = (f32[512]{0:T(512)S(1)}, f32[512]{0:T(512)}, u32[]{:S(2)}) copy-start(f32[512]{0:T(512)} %param.18) | copy-start | bytes 6148
  201.0 1.3 copy-start.2
  203.9 207.6 %all-gather.11.cloned.1.call-start = ((), (), s32[]{:S(2)}) async-start(), calls=%async_computation.7 | async-start | bytes 17301504 | tf_op jit(solution)/shard_map/all_gather | solution.py:104
  204.6 429.8 %all-gather.9.cloned.1.call-start = ((), (), s32[]{:S(2)}) async-start(), calls=%async_computation.6 | async-start | bytes 17301504 | tf_op jit(solution)/shard_map/all_gather | solution.py:99
  205.2 429.2 %copy-start.11 = (f32[2048]{0:T(1024)S(1)}, f32[2048]{0:T(1024)}, u32[]{:S(2)}) copy-start(f32[2048]{0:T(1024)} %param.21) | copy-start | bytes 24580
  218.7 415.7 %copy-start.3 = (bf16[640,2048]{1,0:T(8,128)(2,1)S(1)}, bf16[640,2048]{1,0:T(8,128)(2,1)}, u32[]{:S(2)}) copy-start(bf16[640,2048]{1,0:T(8,128)(2,1)} %all-gather.7.cloned.1.call-done) | copy-start | bytes 7864324
  699.4 1.3 copy-start
Sparse Core Ops, SparseCore 0:
  9.0 148.7 all-gather.4
  204.0 14.6 all-gather.6
  220.3 191.0 all-gather.10
  412.9 221.4 all-gather.8
where the time goes:
time: 709 us
  waiting for transfers between devices  555 us (78%)
  blocking collectives  64.1 us (9%)
  matrix products  42.7 us (6%)
  other arithmetic  17 us (2%)
  between operations  13.3 us (2%)
  starting transfers between devices  8.94 us (1%)
  local copies, waits for them, and re-layouts  7.52 us (1%)
    all_gather x1, waiting for transfers between devices, shards(): lax.all_gather(w_up, 'fs', axis=1, tiled=True)  223 us
    all_gather x1, waiting for transfers between devices, shards(): lax.all_gather(w_down, 'fs', axis=0, tiled=True)  190 us
    all_gather x1, waiting for transfers between devices, side_by_side(): result = lax.all_gather(both, axis, axis=dim, tiled=True)  127 us
    all_to_all x2, blocking collectives, summed_on_arrival(): parts = lax.all_to_all(in_blocks(array, dim, count), axis, 0, 0, tiled=True)  35.1 us
    dot_general x1, matrix products, shards(): jnp.dot(hidden, lax.all_gather(w_down, 'fs', axis=0, tiled=True), preferr...  33.8 us
    psum x1, blocking collectives, shards(): lax.psum((jnp.sum(filtered, axis=1), jnp.sum(filtered * filtered, axis=1)...  22.1 us
  transfers between devices with their start and end apart: 5, of which 4 were waited for; matrix products, arithmetic and copies ran while one was open for 3% of the time, Pallas kernels for 0%

commit v1 on v0

--- a/solution.py
+++ b/solution.py
@@ -5,6 +5,11 @@
 
 KW = 31
 LEN = 128
+
+
+def exchange_gather(block, axis, along):
+    sent = jnp.stack([block] * lax.axis_size(axis))
+    return jnp.concatenate(lax.all_to_all(sent, axis, 0, 0), axis=along)
 
 
 def copy_for_each(array, axis):
@@ -101,7 +106,7 @@
     )
     hidden = jnp.square(jax.nn.relu(up_proj)).astype(jnp.bfloat16)
     feed_partial = jnp.dot(
-        hidden, lax.all_gather(w_down, "fs", axis=0, tiled=True), preferred_element_type=jnp.float32
+        hidden, exchange_gather(w_down, "fs", 0), preferred_element_type=jnp.float32
     )
     feed = summed_on_arrival(feed_partial.astype(jnp.bfloat16), "tp", 1)
     return (second.astype(jnp.float32) + feed).astype(jnp.bfloat16)

time: 709 us -> 723 us (1.020)
  blocking collectives: 64.1 us -> 50.8 us
  waiting for transfers between devices: 555 us -> 568 us
    all_to_all x0 -> x1, waiting for transfers between devices: none -> 300 us  [exchange_gather(): return jnp.concatenate(lax.all_to_all(sent, axis, 0, 0), axis=along)]
    all_gather x1 -> x0, waiting for transfers between devices: 190 us -> none  [shards(): lax.all_gather(w_down, 'fs', axis=0, tiled=True)]
    all_gather x1, waiting for transfers between devices: 223 us -> 139 us  [shards(): lax.all_gather(w_up, 'fs', axis=1, tiled=True)]
    all_to_all x2, blocking collectives: 35.1 us -> 21.7 us  [summed_on_arrival(): parts = lax.all_to_all(in_blocks(array, dim, count), axis, 0, 0, tiled=True)]
    all_gather x1, waiting for transfers between devices: 13.4 us -> 0.84 us  [shards(): gathered_feed = lax.all_gather(second, 'tp', axis=1, tiled=True)]
  transfers between devices with their start and end apart: 5 -> 5, of which waited for: 4 -> 4; matrix products, arithmetic and copies ran while one was open for 3% -> 4% of each run, Pallas kernels for 0% -> 0%
where the time goes in v1:
time: 723 us; the launch traced here: 721 us
  waiting for transfers between devices  568 us (79%)
  blocking collectives  50.8 us (7%)
  matrix products  42.7 us (6%)
  other arithmetic  17 us (2%)
  starting transfers between devices  15.7 us (2%)
  local copies, waits for them, and re-layouts  13.7 us (2%)
  between operations  13.3 us (2%)
    all_to_all x1, waiting for transfers between devices, exchange_gather(): return jnp.concatenate(lax.all_to_all(sent, axis, 0, 0), axis=along)  300 us
    all_gather x1, waiting for transfers between devices, shards(): lax.all_gather(w_up, 'fs', axis=1, tiled=True)  139 us
    all_gather x1, waiting for transfers between devices, side_by_side(): result = lax.all_gather(both, axis, axis=dim, tiled=True)  127 us
    dot_general x1, matrix products, shards(): jnp.dot(hidden, exchange_gather(w_down, 'fs', 0), preferred_element_type=...  33.8 us
    psum x1, blocking collectives, shards(): lax.psum((jnp.sum(filtered, axis=1), jnp.sum(filtered * filtered, axis=1)...  22.1 us
    all_to_all x2, blocking collectives, summed_on_arrival(): parts = lax.all_to_all(in_blocks(array, dim, count), axis, 0, 0, tiled=True)  21.7 us
  transfers between devices with their start and end apart: 5, of which 4 were waited for; matrix products, arithmetic and copies ran while one was open for 4% of the time, Pallas kernels for 0%

profile of v1, /device:TPU:1, one launch (start us, length us, event | category | flops | bytes accessed | tf_op | source)
XLA Modules:
  0.0 721.4 jit_solution(12222752151592111392)
XLA Ops:
  6.5 0.0 all-gather.4.cloned.1.call-start
  6.5 1.5 pad_maximum_fusion
  8.1 0.0 all-gather.4.cloned.1.call-update
  8.1 1.7 copy.15
  9.8 0.2 broadcast_in_dim.4
  10.0 0.0 copy-start.6
  10.0 7.0 all_to_all.25
  17.0 0.0 copy-done.6
  17.0 1.6 broadcast_in_dim.5
  18.6 8.6 %all-to-all-start.1 = ((bf16[32,512,64]{1,2,0:T(8,128)(2,1)}), bf16[32,512,64]{1,2,0:T(8,128)(2,1)}, u32[]{:S(2)}, u32[]{:S(2)}) async-start(bf16[32,512,64]{1,2,0:T(8,128)(2,1)} %broadcast_in_dim.5), calls=%async_computation.1 | async-start | bytes 4194304 | tf_op jit(solution)/shard_map/all_to_all | solution.py:17
  27.3 0.0 copy-start.7
  27.3 0.0 copy-start.8
  27.3 0.0 all-gather.6.cloned.1.call-start
  27.3 0.6 multiply_reduce_fusion
  27.9 0.2 copy-done.7
  28.2 0.0 copy-done.8
  28.2 2.2 fusion.4
  30.4 0.0 copy-start.1
  30.4 127.4 %all-gather.4.cloned.1.call-done = bf16[2048,1024]{1,0:T(8,128)(2,1)} async-done(((bf16[64,1024]{1,0:T(8,128)(2,1)}), bf16[2048,1024]{1,0:T(8,128)(2,1)}) %all-gather.4.cloned.1.call-update) | async-done | bytes 4194320 | tf_op jit(solution)/shard_map/all_gather | solution.py:34
  157.8 0.0 copy-start.4
  157.8 4.2 fusion.28
  162.0 0.0 copy-done.1
  162.0 0.0 copy-done.4
  162.0 0.0 copy-start.9
  162.1 1.6 fusion.16
  163.6 0.0 copy-done.9
  163.7 0.0 copy-start.10
  163.7 0.0 copy-start.11
  163.7 5.5 fusion.93
  169.2 22.1 %all-reduce.1 = (f32[640]{0:T(1024)S(1)}, f32[640]{0:T(1024)S(1)}) all-reduce(f32[640]{0:T(1024)S(1)} %bitcast.78, f32[640]{0:T(1024)S(1)} %bitcast.77), channel_id=1, replica_groups=mesh['rep'=2,'fs'=32,'tp'=2] {'tp'}, use_global_device_ids=true, to_apply=%region_4.5 | all-reduce | flops 1280 | bytes 10240 | tf_op jit(solution)/shard_map/psum | solution.py:89
  191.2 0.0 copy-done.10
  191.2 0.0 copy-done.11
  191.2 0.5 multiply_convert_fusion.1
  191.8 0.0 all-to-all-done.1
  191.8 3.1 convolution_convert_fusion
  194.9 0.3 copy.23
  195.2 5.8 all_to_all.26
  201.0 0.0 copy-start.2
  201.0 0.6 convert_reduce_fusion.1
  201.6 0.7 copy-done.2
  202.3 1.5 add_convert_fusion.1
  203.9 0.0 copy-start.5
  203.9 0.0 all-gather.6.cloned.1.call-update
  203.9 0.0 all-gather.8.cloned.1.call-start
  204.0 0.7 all-gather.8.cloned.1.call-update
  204.7 0.3 copy-done.5
  204.9 5.9 stack.2
  210.9 7.0 all-to-all-start.3
  217.8 0.0 copy-start.12
  217.8 0.8 all-gather.6.cloned.1.call-done
  218.7 0.0 copy-start.3
  218.7 2.5 fusion
  221.2 300.2 %all-to-all-done.3 = bf16[32,128,2048]{2,1,0:T(8,128)(2,1)} async-done(((bf16[32,128,2048]{2,1,0:T(8,128)(2,1)}), bf16[32,128,2048]{2,1,0:T(8,128)(2,1)}, u32[]{:S(2)}, u32[]{:S(2)}) %all-to-all-start.3) | async-done | bytes 16777248 | tf_op jit(solution)/shard_map/all_to_all | solution.py:12
  521.4 139.0 %all-gather.8.cloned.1.call-done = bf16[2048,4096]{1,0:T(8,128)(2,1)} async-done(((bf16[2048,128]{1,0:T(8,128)(2,1)}), bf16[2048,4096]{1,0:T(8,128)(2,1)}) %all-gather.8.cloned.1.call-update) | async-done | bytes 16777232 | tf_op jit(solution)/shard_map/all_gather | solution.py:104
  660.4 0.0 copy-done.12
  660.4 0.0 copy-done.3
  660.4 33.8 %convolution_convert_fusion.1 = bf16[640,2048]{1,0:T(8,128)(2,1)} fusion(bf16[4096,2048]{1,0:T(8,128)(2,1)} %bitcast.42, bf16[2048,4096]{1,0:T(8,128)(2,1)} %all-gather.8.cloned.1.call-done, bf16[640,2048]{1,0:T(8,128)(2,1)S(1)} %copy-done.3, f32[2048]{0:T(1024)S(1)} %copy-done.12, f32[640]{0:T(1024)S(1)} %add_rsqrt_fusion), kind=kOutput, calls=%fused_computation.43 | convolution fusion | flops 21489254400 | bytes 38808064 | tf_op jit(solution)/shard_map/dot_general | solution.py:108
  694.1 2.0 copy.22
  696.1 15.9 %all_to_all.27 = bf16[2,640,1024]{2,1,0:T(8,128)(2,1)S(1)} all-to-all(bf16[2,640,1024]{2,1,0:T(8,128)(2,1)S(1)} %bitcast.72), channel_id=1, replica_groups=mesh['rep'=2,'fs'=32,'tp'=2] {'tp'}, dimensions={0} | all-to-all | bytes 5242880 | tf_op jit(solution)/shard_map/all_to_all | solution.py:46
  712.0 0.0 copy-start
  712.0 0.6 convert_reduce_fusion
  712.6 0.7 copy-done
  713.4 1.5 add_convert_fusion
  (5 shorter events, 0.1 us)
Async XLA Ops:
  6.5 151.2 %all-gather.4.cloned.1.call-start = ((), (), s32[]{:S(2)}) async-start(), calls=%async_computation.5 | async-start | bytes 4325376 | tf_op jit(solution)/shard_map/all_gather | solution.py:34
  10.0 7.0 copy-start.6
  18.6 173.2 %all-to-all-start.1 = ((bf16[32,512,64]{1,2,0:T(8,128)(2,1)}), bf16[32,512,64]{1,2,0:T(8,128)(2,1)}, u32[]{:S(2)}, u32[]{:S(2)}) async-start(bf16[32,512,64]{1,2,0:T(8,128)(2,1)} %broadcast_in_dim.5), calls=%async_computation.1 | async-start | bytes 4194304 | tf_op jit(solution)/shard_map/all_to_all | solution.py:17
  27.3 0.8 copy-start.7
  27.3 0.9 copy-start.8
  27.3 191.4 %all-gather.6.cloned.1.call-start = ((), (), s32[]{:S(2)}) async-start(), calls=%async_computation.6 | async-start | bytes 3932160 | tf_op jit(solution)/shard_map/all_gather | solution.py:100
  30.4 131.7 %copy-start.1 = (bf16[640,2048]{0,1:T(8,128)(2,1)S(1)}, bf16[640,2048]{0,1:T(8,128)(2,1)}, u32[]{:S(2)}) copy-start(bf16[640,2048]{0,1:T(8,128)(2,1)} %fusion.4) | copy-start | bytes 7864324
  157.8 4.3 copy-start.4
  162.0 1.6 copy-start.9
  163.7 27.6 %copy-start.10 = (f32[512]{0:T(512)S(1)}, f32[512]{0:T(512)}, u32[]{:S(2)}) copy-start(f32[512]{0:T(512)} %param.19) | copy-start | bytes 6148
  163.7 27.6 %copy-start.11 = (f32[512]{0:T(512)S(1)}, f32[512]{0:T(512)}, u32[]{:S(2)}) copy-start(f32[512]{0:T(512)} %param.18) | copy-start | bytes 6148
  201.0 1.3 copy-start.2
  203.9 1.0 copy-start.5
  203.9 456.4 %all-gather.8.cloned.1.call-start = ((), (), s32[]{:S(2)}) async-start(), calls=%async_computation.7 | async-start | bytes 17301504 | tf_op jit(solution)/shard_map/all_gather | solution.py:104
  210.9 310.5 %all-to-all-start.3 = ((bf16[32,128,2048]{2,1,0:T(8,128)(2,1)}), bf16[32,128,2048]{2,1,0:T(8,128)(2,1)}, u32[]{:S(2)}, u32[]{:S(2)}) async-start(bf16[32,128,2048]{2,1,0:T(8,128)(2,1)} %stack.2), calls=%async_computation.3 | async-start | bytes 33554432 | tf_op jit(solution)/shard_map/all_to_all | solution.py:12
  217.8 442.5 %copy-start.12 = (f32[2048]{0:T(1024)S(1)}, f32[2048]{0:T(1024)}, u32[]{:S(2)}) copy-start(f32[2048]{0:T(1024)} %param.21) | copy-start | bytes 24580
  218.7 441.7 %copy-start.3 = (bf16[640,2048]{1,0:T(8,128)(2,1)S(1)}, bf16[640,2048]{1,0:T(8,128)(2,1)}, u32[]{:S(2)}) copy-start(bf16[640,2048]{1,0:T(8,128)(2,1)} %all-gather.6.cloned.1.call-done) | copy-start | bytes 7864324
  712.0 1.3 copy-start
Sparse Core Ops, SparseCore 0:
  9.0 148.7 all-gather.3
  204.0 14.6 all-gather.5
  220.3 440.0 all-gather.7
